TPU v7x, 32 devices: a whole 2x2x4 slice. The times are simulated.
32 devices in a mesh: sp: 8 (over z, x), tp: 4 (over y, core).
Axes of the slice: x: 2, y: 2, z: 4, core: 2. Of those that a mesh axis runs over, the one named last changes fastest.
Arguments:
- residual_in: bfloat16 [2048, 2048], P('sp', 'tp'), may hold values from -6 to 6
- conv_input: bfloat16 [2048, 512], P('sp', 'tp'), may hold values from -6 to 6
- outer_gate: bfloat16 [2048, 512], P('sp', 'tp'), may hold values from -6 to 6
- inner_gate: bfloat16 [2048, 512], P('sp', 'tp'), may hold values from -6 to 6
- documents: int32 [2048], P('sp'), may hold values from 0 to 3, as said below
- conv_taps: float32 [3, 512], P(None, 'tp'), may hold values from -3 to 3
- mixer_gain: float32 [512], replicated, may hold values from 0.1 to 1.9
- output_weight: bfloat16 [512, 2048], P(None, 'tp'), may hold values from -0.25 to 0.25
- ffn_gain: float32 [2048], P('tp'), may hold values from 0.1 to 1.9
- routes: int32 [2048, 2], P('sp'), may hold values from 0 to 7, all different within a row; in each aligned block of 256 rows (0 to 255, 256 to 511, ...) at most 128 rows name the same one
- route_weights: float32 [2048, 2], P('sp'), may hold values from 0.1 to 0.9
- expert_gate: bfloat16 [8, 2048, 3584], P('sp', None, 'tp'), may hold values from -0.125 to 0.125
- expert_up: bfloat16 [8, 2048, 3584], P('sp', None, 'tp'), may hold values from -0.125 to 0.125
- expert_down: bfloat16 [8, 3584, 2048], P('sp', 'tp'), may hold values from -0.09375 to 0.09375
Outputs:
- layer_out: bfloat16 [2048, 2048], P('sp', 'tp')
Inputs may be any that keep to these rules, and one draw needn't show every extreme that they name: Document numbers never fall along the positions, and each of the 4 documents occurs. Every document has 256 to 768 positions, and one has exactly 768. `routes`: the two experts of a position differ. Among the 256 positions of one index of sp no expert is named more than 128 times, a bound that some block reaches.
All inputs are finite; a program needn't handle non-finite values.
Results may differ from a plain program's by a relative error of at most 0.0058.
Values may be sent and summed in bfloat16 or wider, within the bound.
A program may use at most 64 MiB of HBM per device.

v0:
```python
import jax
import jax.numpy as jnp
from jax import lax
from jax.sharding import PartitionSpec as P

EPS = 1e-06


def from_behind(block, axis, distance):
    devices = range(lax.axis_size(axis))
    route = [(i - distance, i) for i in devices if i - distance in devices]
    return lax.ppermute(block, axis, route)


def slot_tables(routes, experts, capacity):
    tokens = routes.shape[0]
    flattened = routes.reshape(-1)
    onehot = (flattened[:, None] == jnp.arange(experts, dtype=jnp.int32)[None, :]).astype(jnp.int32)
    earlier = jnp.cumsum(onehot, axis=0) - onehot
    position_in = jnp.sum(earlier * onehot, axis=1)
    target = flattened * capacity + position_in
    owners = (
        jnp.full((experts * capacity,), tokens, jnp.int32)
        .at[target]
        .set(jnp.arange(2 * tokens, dtype=jnp.int32) // 2)
    )
    return (target, owners)


def per_device(
    residual_in,
    conv_input,
    outer_gate,
    inner_gate,
    documents,
    conv_taps,
    mixer_gain,
    output_weight,
    ffn_gain,
    routes,
    route_weights,
    expert_gate,
    expert_up,
    expert_down,
):
    tokens_here = residual_in.shape[0]
    local_features = residual_in.shape[1]
    conv_value = (inner_gate.astype(jnp.float32) * conv_input.astype(jnp.float32)).astype(
        jnp.bfloat16
    )
    doc_marks = documents.astype(jnp.bfloat16)
    before_rows, before_docs = from_behind((conv_value[-2:], doc_marks[-2:]), "sp", 1)
    joined_rows = jnp.concatenate([before_rows, conv_value], axis=0).astype(jnp.float32)
    joined_docs = jnp.concatenate([before_docs, doc_marks], axis=0)
    same_one = (joined_docs[1:-1] == doc_marks).astype(jnp.float32)[:, None]
    same_two = (joined_docs[:-2] == doc_marks).astype(jnp.float32)[:, None]
    conv_sum = (
        conv_taps[2] * joined_rows[2:]
        + conv_taps[1] * joined_rows[1:-1] * same_one
        + conv_taps[0] * joined_rows[:-2] * same_two
    )
    mixed = (outer_gate.astype(jnp.float32) * conv_sum).astype(jnp.bfloat16)
    piece_f = lax.all_gather(mixed, "tp", axis=1, tiled=True).astype(jnp.float32)
    scaled = (piece_f * mixer_gain).astype(jnp.bfloat16)
    accum = jnp.dot(scaled, output_weight, preferred_element_type=jnp.float32)
    squares = jnp.sum(piece_f * piece_f, axis=1)
    mix_scale = lax.rsqrt(squares / mixer_gain.shape[0] + EPS)
    hidden_state = residual_in.astype(jnp.float32) + accum * mix_scale[:, None]
    feature_total = lax.psum(jnp.sum(hidden_state * hidden_state, axis=1), "tp")
    model_width = local_features * lax.axis_size("tp")
    normed = (
        hidden_state * lax.rsqrt(feature_total / model_width + EPS)[:, None] * ffn_gain
    ).astype(jnp.bfloat16)
    experts = lax.axis_size("sp") * expert_gate.shape[0]
    capacity = 4 * tokens_here // experts
    target, owners = slot_tables(routes, experts, capacity)
    padded = jnp.concatenate([normed, jnp.zeros((1, local_features), jnp.bfloat16)], axis=0)
    outgoing = padded[owners].reshape(experts, capacity, local_features)
    slices_in = lax.all_to_all(outgoing, "sp", split_axis=0, concat_axis=0, tiled=True)
    arrived = lax.all_gather(slices_in, "tp", axis=2, tiled=True)
    expert_in = arrived.reshape(-1, model_width)
    gate = jnp.dot(expert_in, expert_gate[0], preferred_element_type=jnp.float32)
    upper = jnp.dot(expert_in, expert_up[0], preferred_element_type=jnp.float32)
    act = (jax.nn.silu(gate) * upper).astype(jnp.bfloat16)
    partial_out = jnp.dot(act, expert_down[0], preferred_element_type=jnp.float32)
    summed = lax.psum_scatter(
        partial_out.astype(jnp.bfloat16), "tp", scatter_dimension=1, tiled=True
    )
    returned = lax.all_to_all(
        summed.reshape(experts, capacity, local_features),
        "sp",
        split_axis=0,
        concat_axis=0,
        tiled=True,
    )
    picked = returned.reshape(experts * capacity, local_features)[target].astype(jnp.float32)
    picked = picked.reshape(tokens_here, 2, local_features)
    routed = jnp.sum(picked * route_weights[:, :, None], axis=1)
    return (hidden_state + routed).astype(jnp.bfloat16)


def solution(mesh):
    placed = (
        P("sp", "tp"),
        P("sp", "tp"),
        P("sp", "tp"),
        P("sp", "tp"),
        P("sp"),
        P(None, "tp"),
        P(),
        P(None, "tp"),
        P("tp"),
        P("sp", None),
        P("sp", None),
        P("sp", None, "tp"),
        P("sp", None, "tp"),
        P("sp", "tp", None),
    )
    return jax.shard_map(
        per_device, mesh=mesh, in_specs=placed, out_specs=P("sp", "tp"), check_vma=False
    )
```

profile of v0, /device:TPU:0, one launch (start us, length us, event | category | flops | bytes accessed | tf_op | source)
XLA Modules:
  0.0 212.3 jit_solution(1286813573739635724)
XLA Ops:
  6.5 0.7 convert_element_type.68
  7.4 4.9 %collective-permute-start.1 = (bf16[2]{0:T(256)(128)(2,1)S(1)}, bf16[2]{0:T(256)(128)(2,1)S(1)}, u32[]{:S(2)}, u32[]{:S(2)}) collective-permute-start(bf16[2]{0:T(256)(128)(2,1)S(1)} %slice.41), channel_id=1, source_target_pairs={{0,4},{4,8},{8,12},{12,16},{16,20},{20,24},{24,28},{1,5},{5,9},{9,... | collective-permute-start | bytes 20 | tf_op jit(solution)/shard_map/ppermute | solution.py:12
  12.2 0.9 multiply_convert_fusion.2
  13.1 3.5 %collective-permute-start = (bf16[2,128]{1,0:T(2,128)(2,1)S(1)}, bf16[2,128]{1,0:T(2,128)(2,1)S(1)}, u32[]{:S(2)}, u32[]{:S(2)}) collective-permute-start(bf16[2,128]{1,0:T(2,128)(2,1)S(1)} %slice.52), channel_id=1, source_target_pairs={{0,4},{4,8},{8,12},{12,16},{16,20},{20,24},{24,28},{1,5},{5,9},{9,... | collective-permute-start | bytes 1544 | tf_op jit(solution)/shard_map/ppermute | solution.py:12
  16.6 0.8 copy.17
  17.4 0.1 eq.37
  17.6 0.1 eq.33
  17.7 0.7 broadcast_multiply_fusion
  18.4 0.8 slice_bitcast_fusion.2
  19.2 1.1 reduce-window.6
  20.3 0.2 slice_reduce_fusion
  20.6 0.1 copy.16
  20.7 0.1 mul.151
  21.0 2.4 %scatter_custom_fusion = s32[1024]{0:T(1024)S(1)} fusion(s32[512]{0:T(512)S(1)} %bitcast.38, s32[512]{0:T(512)S(1)} %add_select_fusion, s32[]{:T(128)} %constant.38.clone.1), kind=kCustom, calls=%fused_computation.49 | custom fusion | bytes 4100 | tf_op jit(solution)/shard_map/scatter | solution.py:25
  23.6 0.8 compare_convert_fusion.1
  24.3 1.0 fusion.15
  25.3 5.8 %all_gather.6 = bf16[256,512]{1,0:T(8,128)(2,1)S(1)} all-gather(bf16[256,128]{1,0:T(8,128)(2,1)S(1)} %fusion.15), channel_id=1, replica_groups=mesh['sp'=8,'tp'=4] {'tp'}, dimensions={1}, use_global_device_ids=true | all-gather | bytes 327680 | tf_op jit(solution)/shard_map/all_gather | solution.py:63
  31.3 1.4 multiply_reduce_fusion.1
  32.7 7.1 %psum.7 = f32[256]{0:T(256)S(1)} all-reduce(f32[256]{0:T(256)S(1)} %get-tuple-element.10), channel_id=1, replica_groups=mesh['sp'=8,'tp'=4] {'tp'}, use_global_device_ids=true, to_apply=%region_2.0 | all-reduce | flops 256 | bytes 2048 | tf_op jit(solution)/shard_map/psum | solution.py:69
  39.9 4.0 %gather_fusion = bf16[1024,512]{1,0:T(8,128)(2,1)S(1)} fusion(bf16[257,512]{1,0:T(8,128)(2,1)S(1)} %concatenate.11, s32[1024]{0:T(1024)S(1)} %fusion.21), kind=kCustom, calls=%fused_computation | custom fusion | bytes 2101248 | tf_op jit(solution)/shard_map/gather | solution.py:78
  43.9 29.1 %all_to_all.10 = bf16[8,128,512]{2,1,0:T(8,128)(2,1)} all-to-all(bf16[8,128,512]{2,1,0:T(8,128)(2,1)S(1)} %bitcast.36), channel_id=1, replica_groups=mesh['sp'=8,'tp'=4] {'sp'}, dimensions={0} | all-to-all | bytes 2097152 | tf_op jit(solution)/shard_map/all_to_all | solution.py:79
  73.1 33.6 %all-gather.2.cloned.1.call-done = bf16[8,128,2048]{2,1,0:T(8,128)(2,1)} async-done(((bf16[8,128,512]{2,1,0:T(8,128)(2,1)}), bf16[8,128,2048]{2,1,0:T(8,128)(2,1)}) %all-gather.2.cloned.1.call-update) | async-done | bytes 4194320 | tf_op jit(solution)/shard_map/all_gather | solution.py:80
  106.6 7.5 %fusion.1 = f32[1024,896]{1,0:T(8,128)S(1)} fusion(bf16[1024,2048]{1,0:T(8,128)(2,1)} %bitcast.41, bf16[1,2048,896]{2,1,0:T(8,128)(2,1)} %param.26), kind=kOutput, calls=%fused_computation.5 | convolution fusion | flops 3758096384 | bytes 11534336 | tf_op jit(solution)/shard_map/dot_general | solution.py:83
  114.2 4.8 %multiply_convert_fusion = bf16[1024,896]{1,0:T(8,128)(2,1)S(1)} fusion(f32[1024,896]{1,0:T(8,128)S(1)} %fusion.1, bf16[1024,2048]{1,0:T(8,128)(2,1)S(1)} %bitcast.42, bf16[1,2048,896]{2,1,0:T(8,128)(2,1)S(1)} %copy-done.4), kind=kOutput, calls=%fused_computation.9 | convolution fusion | flops 3763601408 | bytes 13369344 | tf_op jit(solution)/shard_map/dot_general | solution.py:82
  118.9 6.1 %convolution_convert_fusion = bf16[1024,2048]{1,0:T(8,128)(2,1)} fusion(bf16[1024,896]{1,0:T(8,128)(2,1)S(1)} %multiply_convert_fusion, bf16[1,896,2048]{2,1,0:T(8,128)(2,1)S(1)} %copy-done.5), kind=kOutput, calls=%fused_computation.3 | convolution fusion | flops 3760193536 | bytes 9699328 | tf_op jit(solution)/shard_map/dot_general | solution.py:85
  125.0 44.6 %reduce-scatter.2.cloned.1.call-done = bf16[1024,512]{1,0:T(8,128)(2,1)} async-done(((bf16[1024,2048]{1,0:T(8,128)(2,1)}), bf16[1024,512]{1,0:T(8,128)(2,1)}) %reduce-scatter.2.cloned.1.call-update) | async-done | bytes 1048592 | tf_op jit(solution)/shard_map/reduce_scatter | solution.py:86
  169.6 5.5 %all-to-all-start.1 = ((bf16[8,128,512]{2,1,0:T(8,128)(2,1)}), bf16[8,128,512]{2,1,0:T(8,128)(2,1)S(1)}, u32[]{:S(2)}, u32[]{:S(2)}) async-start(bf16[8,128,512]{2,1,0:T(8,128)(2,1)} %bitcast.37), calls=%async_computation.2 | async-start | bytes 2097152 | tf_op jit(solution)/shard_map/all_to_all | solution.py:89
  175.2 25.5 %all-to-all-done.1 = bf16[8,128,512]{2,1,0:T(8,128)(2,1)S(1)} async-done(((bf16[8,128,512]{2,1,0:T(8,128)(2,1)}), bf16[8,128,512]{2,1,0:T(8,128)(2,1)S(1)}, u32[]{:S(2)}, u32[]{:S(2)}) %all-to-all-start.1) | async-done | bytes 1048608 | tf_op jit(solution)/shard_map/all_to_all | solution.py:89
  200.8 2.0 gather_fusion.1
  202.7 0.7 reshape.78
  203.4 1.3 multiply_reduce_fusion
  204.7 0.8 add_convert_fusion
  (36 shorter events, 0.9 us)
Async XLA Ops:
  6.5 24.8 %copy-start = (bf16[512,512]{1,0:T(8,128)(2,1)S(1)}, bf16[512,512]{1,0:T(8,128)(2,1)}, u32[]{:S(2)}) copy-start(bf16[512,512]{1,0:T(8,128)(2,1)} %param.21) | copy-start | bytes 1572868
  6.5 33.2 %copy-start.1 = (f32[512]{0:T(512)S(1)}, f32[512]{0:T(512)}, u32[]{:S(2)}) copy-start(f32[512]{0:T(512)} %param.22) | copy-start | bytes 6148
  6.5 100.1 %all-gather.2.cloned.1.call-start = ((), (), s32[]{:S(2)}) async-start(), calls=%async_computation.3 | async-start | bytes 5242880 | tf_op jit(solution)/shard_map/all_gather | solution.py:80
  7.4 16.1 %collective-permute-start.1 = (bf16[2]{0:T(256)(128)(2,1)S(1)}, bf16[2]{0:T(256)(128)(2,1)S(1)}, u32[]{:S(2)}, u32[]{:S(2)}) collective-permute-start(bf16[2]{0:T(256)(128)(2,1)S(1)} %slice.41), channel_id=1, source_target_pairs={{0,4},{4,8},{8,12},{12,16},{16,20},{20,24},{24,28},{1,5},{5,9},{9,... | collective-permute-start | bytes 20 | tf_op jit(solution)/shard_map/ppermute | solution.py:12
  13.1 11.2 %collective-permute-start = (bf16[2,128]{1,0:T(2,128)(2,1)S(1)}, bf16[2,128]{1,0:T(2,128)(2,1)S(1)}, u32[]{:S(2)}, u32[]{:S(2)}) collective-permute-start(bf16[2,128]{1,0:T(2,128)(2,1)S(1)} %slice.52), channel_id=1, source_target_pairs={{0,4},{4,8},{8,12},{12,16},{16,20},{20,24},{24,28},{1,5},{5,9},{9,... | collective-permute-start | bytes 1544 | tf_op jit(solution)/shard_map/ppermute | solution.py:12
  73.0 96.6 %reduce-scatter.2.cloned.1.call-start = ((), (), s32[]{:S(2)}) async-start(), calls=%async_computation.4 | async-start | bytes 5242880 | tf_op jit(solution)/shard_map/reduce_scatter | solution.py:86
  106.6 7.5 %copy-start.3 = (bf16[8,128,2048]{2,1,0:T(8,128)(2,1)S(1)}, bf16[8,128,2048]{2,1,0:T(8,128)(2,1)}, u32[]{:S(2)}) copy-start(bf16[8,128,2048]{2,1,0:T(8,128)(2,1)} %all-gather.2.cloned.1.call-done) | copy-start | bytes 12582916
  106.6 7.5 %copy-start.4 = (bf16[1,2048,896]{2,1,0:T(8,128)(2,1)S(1)}, bf16[1,2048,896]{2,1,0:T(8,128)(2,1)}, u32[]{:S(2)}) copy-start(bf16[1,2048,896]{2,1,0:T(8,128)(2,1)} %param.25) | copy-start | bytes 11010052
  114.2 4.8 %copy-start.5 = (bf16[1,896,2048]{2,1,0:T(8,128)(2,1)S(1)}, bf16[1,896,2048]{2,1,0:T(8,128)(2,1)}, u32[]{:S(2)}) copy-start(bf16[1,896,2048]{2,1,0:T(8,128)(2,1)} %param.27) | copy-start | bytes 11010052
  125.0 50.1 %copy-start.2 = (f32[256,2]{0,1:T(2,128)S(1)}, f32[256,2]{0,1:T(2,128)}, u32[]{:S(2)}) copy-start(f32[256,2]{0,1:T(2,128)} %param.24) | copy-start | bytes 6148
  169.6 31.2 %all-to-all-start.1 = ((bf16[8,128,512]{2,1,0:T(8,128)(2,1)}), bf16[8,128,512]{2,1,0:T(8,128)(2,1)S(1)}, u32[]{:S(2)}, u32[]{:S(2)}) async-start(bf16[8,128,512]{2,1,0:T(8,128)(2,1)} %bitcast.37), calls=%async_computation.2 | async-start | bytes 2097152 | tf_op jit(solution)/shard_map/all_to_all | solution.py:89
Sparse Core Ops, SparseCore 0:
  73.1 33.4 all-gather.1
  125.1 44.3 reduce-scatter.1
where the time goes:
time: 213 us; the launch traced here: 212 us
  waiting for transfers between devices  104 us (49%)
  blocking collectives  42 us (20%)
  matrix products  19.7 us (9%)
  starting transfers between devices  13.9 us (7%)
  between operations  13.6 us (6%)
  local copies, waits for them, and re-layouts  11.7 us (5%)
  other arithmetic  7.8 us (4%)
    reduce_scatter x1, waiting for transfers between devices, per_device(): lax.psum_scatter(partial_out.astype(jnp.bfloat16), 'tp', scatter_dimensio...  44.6 us
    all_gather x1, waiting for transfers between devices, per_device(): arrived = lax.all_gather(slices_in, 'tp', axis=2, tiled=True)  33.6 us
    all_to_all x1, blocking collectives, per_device(): lax.all_to_all(outgoing, 'sp', split_axis=0, concat_axis=0, tiled=True)  29.1 us
    all_to_all x1, waiting for transfers between devices, per_device(): lax.all_to_all(summed.reshape(experts, capacity, local_features), 'sp', s...  25.5 us
    ppermute x2, starting transfers between devices, from_behind(): return lax.ppermute(block, axis, route)  8.32 us
    dot_general x1, matrix products, per_device(): upper = jnp.dot(expert_in, expert_up[0], preferred_element_type=jnp.float32)  7.49 us
    psum x1, blocking collectives, per_device(): feature_total = lax.psum(jnp.sum(hidden_state * hidden_state, axis=1), 'tp')  7.09 us
    dot_general x1, matrix products, per_device(): jnp.dot(act, expert_down[0], preferred_element_type=jnp.float32)  6.05 us
  transfers between devices with their start and end apart: 5, of which 3 were waited for; matrix products, arithmetic and copies ran while one was open for 4% of the time, Pallas kernels for 0%

commit v1 on v0

--- a/solution.py
+++ b/solution.py
@@ -1,9 +1,29 @@
+import functools
 import jax
 import jax.numpy as jnp
 from jax import lax
 from jax.sharding import PartitionSpec as P
 
 EPS = 1e-06
+
+
+def perform_sources_all_all(sample, shard_axis):
+    many = lax.axis_size(shard_axis)
+    windows = []
+    for dd in range(1, many):
+        windows.append((dd - 1, dd))
+    r1 = windows + [(many - 1, 0)]
+    back = sample
+    cards = [back]
+    for _ in range(many - 1):
+        back = lax.ppermute(back, shard_axis, r1)
+        cards += [back]
+    low = jnp.concatenate([*reversed(cards)], axis=2)
+    reply = lax.axis_index(shard_axis)
+    return jnp.roll(low, (reply + 1) * back.shape[2], 2)
+
+
+measure_the_keys = functools.partial(perform_sources_all_all, shard_axis="tp")
 
 
 def from_behind(block, axis, distance):
@@ -77,7 +97,7 @@
     padded = jnp.concatenate([normed, jnp.zeros((1, local_features), jnp.bfloat16)], axis=0)
     outgoing = padded[owners].reshape(experts, capacity, local_features)
     slices_in = lax.all_to_all(outgoing, "sp", split_axis=0, concat_axis=0, tiled=True)
-    arrived = lax.all_gather(slices_in, "tp", axis=2, tiled=True)
+    arrived = measure_the_keys(slices_in)
     expert_in = arrived.reshape(-1, model_width)
     gate = jnp.dot(expert_in, expert_gate[0], preferred_element_type=jnp.float32)
     upper = jnp.dot(expert_in, expert_up[0], preferred_element_type=jnp.float32)

time: 213 us -> 227 us (1.066)
  local copies, waits for them, and re-layouts: 11.7 us -> 19.8 us
  waiting for transfers between devices: 104 us -> 112 us
  matrix products: 19.7 us -> 16.6 us
    ppermute x0 -> x3, waiting for transfers between devices: none -> 43.1 us  [perform_sources_all_all(): back = lax.ppermute(back, shard_axis, r1)]
    all_gather x1 -> x0, waiting for transfers between devices: 33.6 us -> none  [per_device(): arrived = lax.all_gather(slices_in, 'tp', axis=2, tiled=True)]
    unnamed x14 -> x19, local copies, waits for them, and re-layouts: 0.97 us -> 8.65 us
    dot_general x1, matrix products: 7.49 us -> 4.69 us  [per_device(): upper = jnp.dot(expert_in, expert_up[0], preferred_element_type=jnp.float32)]
  transfers between devices with their start and end apart: 5 -> 7, of which waited for: 3 -> 5; matrix products, arithmetic and copies ran while one was open for 4% -> 4% of each run, Pallas kernels for 0% -> 0%
where the time goes in v1:
time: 227 us
  waiting for transfers between devices  112 us (49%)
  blocking collectives  41.9 us (18%)
  local copies, waits for them, and re-layouts  19.8 us (9%)
  matrix products  16.6 us (7%)
  starting transfers between devices  13.8 us (6%)
  between operations  13.7 us (6%)
  other arithmetic  8.49 us (4%)
    reduce_scatter x1, waiting for transfers between devices, per_device(): lax.psum_scatter(partial_out.astype(jnp.bfloat16), 'tp', scatter_dimensio...  43.6 us
    ppermute x3, waiting for transfers between devices, perform_sources_all_all(): back = lax.ppermute(back, shard_axis, r1)  43.1 us
    all_to_all x1, blocking collectives, per_device(): lax.all_to_all(outgoing, 'sp', split_axis=0, concat_axis=0, tiled=True)  29 us
    all_to_all x1, waiting for transfers between devices, per_device(): lax.all_to_all(summed.reshape(experts, capacity, local_features), 'sp', s...  25.5 us
    unnamed x19, local copies, waits for them, and re-layouts  8.65 us
    ppermute x2, starting transfers between devices, from_behind(): return lax.ppermute(block, axis, route)  8.32 us
    psum x1, blocking collectives, per_device(): feature_total = lax.psum(jnp.sum(hidden_state * hidden_state, axis=1), 'tp')  7.1 us
    dot_general x1, matrix products, per_device(): jnp.dot(act, expert_down[0], preferred_element_type=jnp.float32)  6.08 us
  transfers between devices with their start and end apart: 7, of which 5 were waited for; matrix products, arithmetic and copies ran while one was open for 4% of the time, Pallas kernels for 0%

profile of v1, /device:TPU:0, one launch (start us, length us, event | category | flops | bytes accessed | tf_op | source)
XLA Modules:
  0.0 226.5 jit_solution(12594228489039411789)
XLA Ops:
  7.4 4.9 %collective-permute-start.1 = (bf16[2]{0:T(256)(128)(2,1)S(1)}, bf16[2]{0:T(256)(128)(2,1)S(1)}, u32[]{:S(2)}, u32[]{:S(2)}) collective-permute-start(bf16[2]{0:T(256)(128)(2,1)S(1)} %slice.41), channel_id=1, source_target_pairs={{0,4},{4,8},{8,12},{12,16},{16,20},{20,24},{24,28},{1,5},{5,9},{9,... | collective-permute-start | bytes 20 | tf_op jit(solution)/shard_map/ppermute | solution.py:32
  12.2 0.9 multiply_convert_fusion.2
  13.1 3.5 %collective-permute-start = (bf16[2,128]{1,0:T(2,128)(2,1)S(1)}, bf16[2,128]{1,0:T(2,128)(2,1)S(1)}, u32[]{:S(2)}, u32[]{:S(2)}) collective-permute-start(bf16[2,128]{1,0:T(2,128)(2,1)S(1)} %slice.52), channel_id=1, source_target_pairs={{0,4},{4,8},{8,12},{12,16},{16,20},{20,24},{24,28},{1,5},{5,9},{9,... | collective-permute-start | bytes 1544 | tf_op jit(solution)/shard_map/ppermute | solution.py:32
  16.6 0.8 copy.17
  18.4 0.8 slice_bitcast_fusion.2
  19.2 1.1 reduce-window.6
  21.0 2.4 %scatter_custom_fusion = s32[1024]{0:T(1024)S(1)} fusion(s32[512]{0:T(512)S(1)} %bitcast.40, s32[512]{0:T(512)S(1)} %add_select_fusion, s32[]{:T(128)} %constant.61.clone.1), kind=kCustom, calls=%fused_computation.57 | custom fusion | bytes 4100 | tf_op jit(solution)/shard_map/scatter | solution.py:45
  23.5 0.8 compare_convert_fusion.1
  24.3 1.0 fusion.15
  25.3 5.8 %all_gather.3 = bf16[256,512]{1,0:T(8,128)(2,1)S(1)} all-gather(bf16[256,128]{1,0:T(8,128)(2,1)S(1)} %fusion.15), channel_id=1, replica_groups=mesh['sp'=8,'tp'=4] {'tp'}, dimensions={1}, use_global_device_ids=true | all-gather | bytes 327680 | tf_op jit(solution)/shard_map/all_gather | solution.py:83
  31.3 1.4 multiply_reduce_fusion.1
  32.7 7.1 %psum.7 = f32[256]{0:T(256)S(1)} all-reduce(f32[256]{0:T(256)S(1)} %get-tuple-element.10), channel_id=1, replica_groups=mesh['sp'=8,'tp'=4] {'tp'}, use_global_device_ids=true, to_apply=%region_2.0 | all-reduce | flops 256 | bytes 2048 | tf_op jit(solution)/shard_map/psum | solution.py:89
  39.8 0.8 multiply_convert_fusion.1
  40.6 4.0 %gather_fusion = bf16[1024,512]{1,0:T(8,128)(2,1)S(1)} fusion(bf16[257,512]{1,0:T(8,128)(2,1)S(1)} %concatenate.17, s32[1024]{0:T(1024)S(1)} %fusion.21), kind=kCustom, calls=%fused_computation | custom fusion | bytes 2101248 | tf_op jit(solution)/shard_map/gather | solution.py:98
  44.6 29.0 %all_to_all.10 = bf16[8,128,512]{2,1,0:T(8,128)(2,1)S(1)} all-to-all(bf16[8,128,512]{2,1,0:T(8,128)(2,1)S(1)} %bitcast.36), channel_id=1, replica_groups=mesh['sp'=8,'tp'=4] {'sp'}, dimensions={0} | all-to-all | bytes 2097152 | tf_op jit(solution)/shard_map/all_to_all | solution.py:99
  73.5 14.2 %collective-permute-done.2 = bf16[8,128,512]{2,1,0:T(8,128)(2,1)S(1)} collective-permute-done((bf16[8,128,512]{2,1,0:T(8,128)(2,1)S(1)}, bf16[8,128,512]{2,1,0:T(8,128)(2,1)S(1)}, u32[]{:S(2)}, u32[]{:S(2)}) %collective-permute-start.2) | collective-permute-done | bytes 1048608 | tf_op jit(solution)/shard_map/ppermute | solution.py:19
  87.8 14.3 %collective-permute-done.3 = bf16[8,128,512]{2,1,0:T(8,128)(2,1)} collective-permute-done((bf16[8,128,512]{2,1,0:T(8,128)(2,1)S(1)}, bf16[8,128,512]{2,1,0:T(8,128)(2,1)}, u32[]{:S(2)}, u32[]{:S(2)}) %collective-permute-start.3) | collective-permute-done | bytes 1048608 | tf_op jit(solution)/shard_map/ppermute | solution.py:19
  102.1 14.5 %collective-permute-done.4 = bf16[8,128,512]{2,1,0:T(8,128)(2,1)} collective-permute-done((bf16[8,128,512]{2,1,0:T(8,128)(2,1)}, bf16[8,128,512]{2,1,0:T(8,128)(2,1)}, u32[]{:S(2)}, u32[]{:S(2)}) %collective-permute-start.4) | collective-permute-done | bytes 1048608 | tf_op jit(solution)/shard_map/ppermute | solution.py:19
  116.6 1.4 constant_dynamic-update-slice_fusion.7
  118.0 1.4 constant_dynamic-update-slice_fusion.6
  119.7 1.4 constant_dynamic-update-slice_fusion.3
  121.1 1.4 constant_dynamic-update-slice_fusion.2
  123.2 1.7 copy-done.2
  124.9 4.5 %fusion.3 = f32[1024,896]{1,0:T(8,128)S(1)} fusion(bf16[1024,2048]{1,0:T(8,128)(2,1)S(1)} %bitcast.37, bf16[1,2048,896]{2,1,0:T(8,128)(2,1)S(1)} %copy-done.2), kind=kOutput, calls=%fused_computation.7 | convolution fusion | flops 3758096384 | bytes 11534336 | tf_op jit(solution)/shard_map/dot_general | solution.py:102
  129.4 4.7 %multiply_convert_fusion = bf16[1024,896]{1,0:T(8,128)(2,1)S(1)} fusion(f32[1024,896]{1,0:T(8,128)S(1)} %fusion.3, bf16[1024,2048]{1,0:T(8,128)(2,1)S(1)} %bitcast.38, bf16[1,2048,896]{2,1,0:T(8,128)(2,1)S(1)} %copy-done.3), kind=kOutput, calls=%fused_computation.9 | convolution fusion | flops 3763601408 | bytes 13369344 | tf_op jit(solution)/shard_map/dot_general | solution.py:103
  134.1 6.1 %convolution_convert_fusion = bf16[1024,2048]{1,0:T(8,128)(2,1)} fusion(bf16[1024,896]{1,0:T(8,128)(2,1)S(1)} %multiply_convert_fusion, bf16[1,896,2048]{2,1,0:T(8,128)(2,1)S(1)} %copy-done.4), kind=kOutput, calls=%fused_computation.3 | convolution fusion | flops 3760193536 | bytes 9699328 | tf_op jit(solution)/shard_map/dot_general | solution.py:105
  140.2 43.6 %reduce-scatter.2.cloned.1.call-done = bf16[1024,512]{1,0:T(8,128)(2,1)} async-done(((bf16[1024,2048]{1,0:T(8,128)(2,1)}), bf16[1024,512]{1,0:T(8,128)(2,1)}) %reduce-scatter.2.cloned.1.call-update) | async-done | bytes 1048592 | tf_op jit(solution)/shard_map/reduce_scatter | solution.py:106
  183.8 5.5 %all-to-all-start.1 = ((bf16[8,128,512]{2,1,0:T(8,128)(2,1)}), bf16[8,128,512]{2,1,0:T(8,128)(2,1)S(1)}, u32[]{:S(2)}, u32[]{:S(2)}) async-start(bf16[8,128,512]{2,1,0:T(8,128)(2,1)} %bitcast.39), calls=%async_computation.2 | async-start | bytes 2097152 | tf_op jit(solution)/shard_map/all_to_all | solution.py:109
  189.5 25.5 %all-to-all-done.1 = bf16[8,128,512]{2,1,0:T(8,128)(2,1)S(1)} async-done(((bf16[8,128,512]{2,1,0:T(8,128)(2,1)}), bf16[8,128,512]{2,1,0:T(8,128)(2,1)S(1)}, u32[]{:S(2)}, u32[]{:S(2)}) %all-to-all-start.1) | async-done | bytes 1048608 | tf_op jit(solution)/shard_map/all_to_all | solution.py:109
  215.0 2.0 gather_fusion.1
  217.6 1.3 multiply_reduce_fusion
  218.9 0.8 add_convert_fusion
  (46 shorter events, 4.5 us)
Async XLA Ops:
  6.5 24.8 %copy-start = (bf16[512,512]{1,0:T(8,128)(2,1)S(1)}, bf16[512,512]{1,0:T(8,128)(2,1)}, u32[]{:S(2)}) copy-start(bf16[512,512]{1,0:T(8,128)(2,1)} %param.21) | copy-start | bytes 1572868
  6.5 177.2 %reduce-scatter.2.cloned.1.call-start = ((), (), s32[]{:S(2)}) async-start(), calls=%async_computation.3 | async-start | bytes 5242880 | tf_op jit(solution)/shard_map/reduce_scatter | solution.py:106
  7.4 16.1 %collective-permute-start.1 = (bf16[2]{0:T(256)(128)(2,1)S(1)}, bf16[2]{0:T(256)(128)(2,1)S(1)}, u32[]{:S(2)}, u32[]{:S(2)}) collective-permute-start(bf16[2]{0:T(256)(128)(2,1)S(1)} %slice.41), channel_id=1, source_target_pairs={{0,4},{4,8},{8,12},{12,16},{16,20},{20,24},{24,28},{1,5},{5,9},{9,... | collective-permute-start | bytes 20 | tf_op jit(solution)/shard_map/ppermute | solution.py:32
  13.1 11.2 %collective-permute-start = (bf16[2,128]{1,0:T(2,128)(2,1)S(1)}, bf16[2,128]{1,0:T(2,128)(2,1)S(1)}, u32[]{:S(2)}, u32[]{:S(2)}) collective-permute-start(bf16[2,128]{1,0:T(2,128)(2,1)S(1)} %slice.52), channel_id=1, source_target_pairs={{0,4},{4,8},{8,12},{12,16},{16,20},{20,24},{24,28},{1,5},{5,9},{9,... | collective-permute-start | bytes 1544 | tf_op jit(solution)/shard_map/ppermute | solution.py:32
  73.5 14.2 %collective-permute-start.2 = (bf16[8,128,512]{2,1,0:T(8,128)(2,1)S(1)}, bf16[8,128,512]{2,1,0:T(8,128)(2,1)S(1)}, u32[]{:S(2)}, u32[]{:S(2)}) collective-permute-start(bf16[8,128,512]{2,1,0:T(8,128)(2,1)S(1)} %all_to_all.10), channel_id=1, source_target_pairs={{0,1},{1,2},{2,3},{3,0},{4,5},{5,6},{6,7},{7,4},{8,9},{9,10},{10,1... | collective-permute-start | bytes 3145736 | tf_op jit(solution)/shard_map/ppermute | solution.py:19
  87.8 14.3 %collective-permute-start.3 = (bf16[8,128,512]{2,1,0:T(8,128)(2,1)S(1)}, bf16[8,128,512]{2,1,0:T(8,128)(2,1)}, u32[]{:S(2)}, u32[]{:S(2)}) collective-permute-start(bf16[8,128,512]{2,1,0:T(8,128)(2,1)S(1)} %collective-permute-done.2), channel_id=1, source_target_pairs={{0,1},{1,2},{2,3},{3,0},{4,5},{5,6},{6,7},{7,4},{8,9},{9,10},{10,1... | collective-permute-start | bytes 3145736 | tf_op jit(solution)/shard_map/ppermute | solution.py:19
  102.1 14.5 %collective-permute-start.4 = (bf16[8,128,512]{2,1,0:T(8,128)(2,1)}, bf16[8,128,512]{2,1,0:T(8,128)(2,1)}, u32[]{:S(2)}, u32[]{:S(2)}) collective-permute-start(bf16[8,128,512]{2,1,0:T(8,128)(2,1)} %collective-permute-done.3), channel_id=1, source_target_pairs={{0,1},{1,2},{2,3},{3,0},{4,5},{5,6},{6,7},{7,4},{8,9},{9,10},{10,1... | collective-permute-start | bytes 3145736 | tf_op jit(solution)/shard_map/ppermute | solution.py:19
  122.8 2.0 copy-start.2
  124.9 4.5 %copy-start.3 = (bf16[1,2048,896]{2,1,0:T(8,128)(2,1)S(1)}, bf16[1,2048,896]{2,1,0:T(8,128)(2,1)}, u32[]{:S(2)}) copy-start(bf16[1,2048,896]{2,1,0:T(8,128)(2,1)} %param.26) | copy-start | bytes 11010052
  129.4 4.7 %copy-start.4 = (bf16[1,896,2048]{2,1,0:T(8,128)(2,1)S(1)}, bf16[1,896,2048]{2,1,0:T(8,128)(2,1)}, u32[]{:S(2)}) copy-start(bf16[1,896,2048]{2,1,0:T(8,128)(2,1)} %param.27) | copy-start | bytes 11010052
  140.2 49.1 %copy-start.1 = (f32[256,2]{0,1:T(2,128)S(1)}, f32[256,2]{0,1:T(2,128)}, u32[]{:S(2)}) copy-start(f32[256,2]{0,1:T(2,128)} %param.24) | copy-start | bytes 6148
  183.8 31.2 %all-to-all-start.1 = ((bf16[8,128,512]{2,1,0:T(8,128)(2,1)}), bf16[8,128,512]{2,1,0:T(8,128)(2,1)S(1)}, u32[]{:S(2)}, u32[]{:S(2)}) async-start(bf16[8,128,512]{2,1,0:T(8,128)(2,1)} %bitcast.39), calls=%async_computation.2 | async-start | bytes 2097152 | tf_op jit(solution)/shard_map/all_to_all | solution.py:109
Sparse Core Ops, SparseCore 0:
  140.3 43.4 reduce-scatter.1
